TPU v7x, 256 devices: a whole 4x4x8 slice. The times are simulated.
256 devices in a mesh: rep: 2 (over z_hi), fs: 16 (over z_lo, y), tp: 8 (over x, core).
Axes of the slice: x: 4, y: 4, z: 8 (z_hi: 2, z_lo: 4; z = z_hi * 4 + z_lo), core: 2. Of those that a mesh axis runs over, the one named last changes fastest.
Arguments:
- stream: bfloat16 [16384, 2048], P(('rep', 'fs'), 'tp'), may hold values from -6 to 6
- recurrent_norm_gain: float32 [2048], replicated, may hold values from 0.1 to 1.9
- feedforward_norm_gain: float32 [2048], replicated, may hold values from 0.1 to 1.9
- recurrent_input_weight: bfloat16 [2048, 2048], P('fs', 'tp'), may hold values from -0.125 to 0.125
- output_gate_weight: bfloat16 [2048, 2048], P('fs', 'tp'), may hold values from -0.125 to 0.125
- causal_filter_weight: bfloat16 [4, 2048], P(None, 'tp'), may hold values from -3 to 3
- decay_gate_matrix: bfloat16 [32, 64, 64], P('tp'), may hold values from -0.75 to 0.75
- input_gate_matrix: bfloat16 [32, 64, 64], P('tp'), may hold values from -0.75 to 0.75
- channel_decay_param: float32 [2048], P('tp'), may hold values from 3 to 10
- token_decay_offset: float32 [16384, 2048], P(('rep', 'fs'), 'tp'), may hold values from -0.7 to 0, as said below
- recurrent_output_weight: bfloat16 [2048, 2048], P('tp', 'fs'), may hold values from -0.125 to 0.125
- up_projection_weight: bfloat16 [2048, 6144], P('fs', 'tp'), may hold values from -0.125 to 0.125
- down_projection_weight: bfloat16 [6144, 2048], P('tp', 'fs'), may hold values from -0.078125 to 0.078125
Outputs:
- updated: bfloat16 [16384, 2048], P(('rep', 'fs'), 'tp')
Inputs may be any that keep to these rules, and one draw needn't show every extreme that they name: `token_decay_offset`: zero except at a few positions, where a whole row is negative.
All inputs are finite; a program needn't handle non-finite values.
Results may differ from a plain program's by a relative error of at most 0.015.
Values may be sent and summed in bfloat16 or wider, within the bound.
A program may use at most 64 MiB of HBM per device.

v0:
```python
import jax
import jax.numpy as jnp
from jax import lax
from jax.sharding import Mesh
from jax.sharding import PartitionSpec as P

SEQ_LEN = 128
FS = ("fs_0", "fs_1")
REP_FS = ("rep", "fs_0", "fs_1")
EPSILON = 1e-06
DECAY_MULTIPLIER = 8.0


def in_order(pieces, dim):
    shape = list(pieces.shape[1:])
    shape[dim] *= pieces.shape[0]
    return jnp.moveaxis(pieces, 0, dim).reshape(shape)


def from_everyone(value, axis):
    copies = jnp.broadcast_to(value, (lax.axis_size(axis), *value.shape))
    return lax.all_to_all(copies, axis, split_axis=0, concat_axis=0, tiled=True)


def gather_directly(value, axis, dim):
    return in_order(from_everyone(value, axis), dim)


def in_one_piece(arrays, axis, dim, along):
    ends, at = ([], 0)
    for a in arrays[:-1]:
        at += a.shape[along]
        ends.append(at)
    both = jnp.concatenate(arrays, axis=along)
    return tuple(jnp.split(lax.all_gather(both, axis, axis=dim, tiled=True), ends, axis=along))


def split_up(value, dim, devices):
    before, after = (value.shape[:dim], value.shape[dim + 1 :])
    return jnp.moveaxis(value.reshape(*before, devices, -1, *after), dim, 0)


def sent_and_summed(value, axis, dim):
    pieces = split_up(value, dim, lax.axis_size(axis))
    arrived = lax.all_to_all(pieces, axis, split_axis=0, concat_axis=0, tiled=True)
    return arrived.astype(jnp.float32).sum(axis=0)


def gather_in_order(value, axes, order):
    pieces = value[None]
    for k in order:
        pieces = lax.all_gather(pieces, axes[k], axis=0, tiled=True)
    held = [lax.axis_size(axes[k]) for k in reversed(order)]
    pieces = pieces.reshape(*held, *value.shape)
    turned = sorted(range(len(order)), key=lambda place: order[len(order) - 1 - place])
    return pieces.transpose(*turned, *range(len(order), pieces.ndim)).reshape(-1, *value.shape)


def gather_axes(value, axes, order, dim):
    return in_order(gather_in_order(value, axes, order), dim)


def norm_rows(values, gain):
    widened = values.astype(jnp.float32)
    inverse = lax.rsqrt(jnp.mean(widened * widened, axis=-1, keepdims=True) + EPSILON)
    return (widened * inverse * gain).astype(jnp.bfloat16)


def short_filter(values, causal_filter_weight, sequence_length):
    positions, channels = values.shape
    sequences = positions // sequence_length
    reach = causal_filter_weight.shape[0]
    widened = (
        lax.optimization_barrier(values)
        .astype(jnp.float32)
        .reshape(sequences, sequence_length, channels)
    )
    padded = jnp.pad(widened, ((0, 0), (reach - 1, 0), (0, 0)))
    taps = causal_filter_weight.astype(jnp.float32)
    total = taps[0] * padded[:, 0:sequence_length]
    for offset in range(1, reach):
        total = total + taps[offset] * padded[:, offset : offset + sequence_length]
    return total.reshape(positions, channels).astype(jnp.bfloat16)


def combine(earlier, later):
    return (earlier[0] * later[0], later[0] * earlier[1] + later[1])


def recurrent_states(
    filtered_input,
    output_gate_rows,
    decay_gate_matrix,
    input_gate_matrix,
    channel_decay_param,
    token_decay_offset,
    sequence_length,
):
    positions, channels = filtered_input.shape
    blocks, block_size, _ = decay_gate_matrix.shape
    grouped = filtered_input.reshape(positions, blocks, block_size)
    recurrent_step = jax.nn.sigmoid(
        jnp.einsum(
            "tnc,ncd->tnd", grouped, decay_gate_matrix, preferred_element_type=jnp.float32
        ).reshape(positions, channels)
    )
    inputs = jax.nn.sigmoid(
        jnp.einsum(
            "tnc,ncd->tnd", grouped, input_gate_matrix, preferred_element_type=jnp.float32
        ).reshape(positions, channels)
    )
    decay_logarithm = (
        -DECAY_MULTIPLIER * recurrent_step * jax.nn.softplus(-channel_decay_param)
        + token_decay_offset
    )
    widened = lax.optimization_barrier(filtered_input).astype(jnp.float32)
    drive = jnp.sqrt(-jnp.expm1(2.0 * decay_logarithm)) * inputs * widened
    shaped = (positions // sequence_length, sequence_length, channels)
    _, states = lax.associative_scan(
        combine, (jnp.exp(decay_logarithm).reshape(shaped), drive.reshape(shaped)), axis=1
    )
    gate_wide = lax.optimization_barrier(output_gate_rows).astype(jnp.float32)
    return (states.reshape(positions, channels) * jax.nn.gelu(gate_wide, approximate=False)).astype(
        jnp.bfloat16
    )


def shards(
    stream,
    recurrent_norm_gain,
    feedforward_norm_gain,
    recurrent_input_weight,
    output_gate_weight,
    causal_filter_weight,
    decay_gate_matrix,
    input_gate_matrix,
    channel_decay_param,
    token_decay_offset,
    recurrent_output_weight,
    up_projection_weight,
    down_projection_weight,
):
    whole = gather_directly(stream, "tp", 1)
    normed = norm_rows(whole, recurrent_norm_gain)
    pieces = in_one_piece((recurrent_input_weight, output_gate_weight), FS, 0, 1)
    columns = normed
    value_total = jnp.dot(columns, pieces[0], preferred_element_type=jnp.float32)
    gate_total = jnp.dot(columns, pieces[1], preferred_element_type=jnp.float32)
    filtered_input = short_filter(value_total.astype(jnp.bfloat16), causal_filter_weight, SEQ_LEN)
    mixed_rows = recurrent_states(
        filtered_input,
        gate_total.astype(jnp.bfloat16),
        decay_gate_matrix,
        input_gate_matrix,
        channel_decay_param,
        token_decay_offset,
        SEQ_LEN,
    )
    mixer_terms = jnp.dot(
        mixed_rows,
        gather_directly(recurrent_output_weight, FS, 1),
        preferred_element_type=jnp.float32,
    )
    summed = sent_and_summed(mixer_terms.astype(jnp.bfloat16), "tp", 1)
    middle = (stream.astype(jnp.float32) + summed).astype(jnp.bfloat16)
    whole_mid = gather_directly(middle, "tp", 1)
    normed_mid = norm_rows(whole_mid, feedforward_norm_gain)
    columns = normed_mid
    raised = jnp.dot(
        columns,
        gather_axes(up_projection_weight, FS, (0, 1), 0),
        preferred_element_type=jnp.float32,
    )
    activity = jnp.square(jax.nn.relu(raised)).astype(jnp.bfloat16)
    channel_terms = jnp.dot(
        activity,
        gather_axes(down_projection_weight, FS, (0, 1), 1),
        preferred_element_type=jnp.float32,
    )
    channel_sum = sent_and_summed(channel_terms.astype(jnp.bfloat16), "tp", 1)
    return (middle.astype(jnp.float32) + channel_sum).astype(jnp.bfloat16)


def solution(mesh):
    split = Mesh(
        mesh.devices.reshape(mesh.shape["rep"], 4, 4, mesh.shape["tp"]),
        ("rep", "fs_0", "fs_1", "tp"),
    )
    placed = (
        P(REP_FS, "tp"),
        P(),
        P(),
        P(FS, "tp"),
        P(FS, "tp"),
        P(None, "tp"),
        P("tp", None, None),
        P("tp", None, None),
        P("tp"),
        P(REP_FS, "tp"),
        P("tp", FS),
        P(FS, "tp"),
        P("tp", FS),
    )
    return jax.shard_map(
        shards, mesh=split, in_specs=placed, out_specs=P(REP_FS, "tp"), check_vma=False
    )
```

profile of v0, /device:TPU:1, one launch (start us, length us, event | category | flops | bytes accessed | tf_op | source)
XLA Modules:
  0.0 238.8 jit_solution(2918589249318210032)
XLA Ops:
  6.5 1.6 pad_maximum_fusion.1
  8.2 19.7 %all-gather.1 = bf16[3072,128]{1,0:T(8,128)(2,1)} all-gather(bf16[768,128]{1,0:T(8,128)(2,1)} %param.25), channel_id=3, replica_groups=mesh['rep'=2,'fs_0'=4,'fs_1'=4,'tp'=8] {'fs_0'}, dimensions={0}, use_global_device_ids=true | all-gather | bytes 983040 | tf_op jit(solution)/shard_map/all_gather | solution.py:52
  28.1 1.6 broadcast_in_dim.20
  29.6 8.2 %all-to-all-start = ((bf16[8,512,256]{1,2,0:T(8,128)(2,1)}), bf16[8,512,256]{1,2,0:T(8,128)(2,1)S(1)}, u32[]{:S(2)}, u32[]{:S(2)}) async-start(bf16[8,512,256]{1,2,0:T(8,128)(2,1)} %broadcast_in_dim.20), calls=%async_computation | async-start | bytes 4194304 | tf_op jit(solution)/shard_map/all_to_all | solution.py:22
  37.9 22.9 %all-gather = bf16[512,768]{1,0:T(8,128)(2,1)} all-gather(bf16[128,768]{1,0:T(8,128)(2,1)S(1)} %copy-done.3), channel_id=2, replica_groups=mesh['rep'=2,'fs_0'=4,'fs_1'=4,'tp'=8] {'fs_0'}, dimensions={0}, use_global_device_ids=true | all-gather | bytes 983040 | tf_op jit(solution)/shard_map/all_gather | solution.py:52
  61.0 3.2 %all-to-all-done = bf16[8,512,256]{1,2,0:T(8,128)(2,1)S(1)} async-done(((bf16[8,512,256]{1,2,0:T(8,128)(2,1)}), bf16[8,512,256]{1,2,0:T(8,128)(2,1)S(1)}, u32[]{:S(2)}, u32[]{:S(2)}) %all-to-all-start) | async-done | bytes 2097184 | tf_op jit(solution)/shard_map/all_to_all | solution.py:22
  64.2 1.1 broadcast_in_dim.21
  65.3 6.7 %all-to-all-start.1 = ((bf16[16,256,128]{1,2,0:T(8,128)(2,1)}), bf16[16,256,128]{1,2,0:T(8,128)(2,1)S(1)}, u32[]{:S(2)}, u32[]{:S(2)}) async-start(bf16[16,256,128]{1,2,0:T(8,128)(2,1)} %broadcast_in_dim.21), calls=%async_computation.1 | async-start | bytes 2097152 | tf_op jit(solution)/shard_map/all_to_all | solution.py:22
  72.0 0.5 multiply_reduce_fusion
  72.5 1.9 fusion.4
  74.4 15.4 %all-gather.6.cloned.1.call-done = bf16[2048,512]{1,0:T(8,128)(2,1)} async-done(((bf16[128,512]{1,0:T(8,128)(2,1)}), bf16[2048,512]{1,0:T(8,128)(2,1)}) %all-gather.6.cloned.1.call-update) | async-done | bytes 2097168 | tf_op jit(solution)/shard_map/all_gather | solution.py:35
  89.8 2.6 %convolution_convert_fusion.3 = bf16[512,256]{1,0:T(8,128)(2,1)S(1)} fusion(bf16[512,2048]{0,1:T(8,128)(2,1)} %fusion.4, bf16[2048,512]{1,0:T(8,128)(2,1)} %all-gather.6.cloned.1.call-done), kind=kOutput, calls=%fused_computation.25 | convolution fusion | flops 537001984 | bytes 3407872 | tf_op jit(solution)/shard_map/dot_general | solution.py:147
  93.0 0.3 fusion.8
  94.3 1.5 fusion.47
  96.2 0.8 slice.194
  97.0 1.0 fusion.57
  100.8 2.6 %convolution_convert_fusion.2 = bf16[512,256]{1,0:T(8,128)(2,1)S(1)} fusion(bf16[512,2048]{0,1:T(8,128)(2,1)} %fusion.4, bf16[2048,512]{1,0:T(8,128)(2,1)} %all-gather.6.cloned.1.call-done), kind=kOutput, calls=%fused_computation.24 | convolution fusion | flops 537001984 | bytes 3407872 | tf_op jit(solution)/shard_map/dot_general | solution.py:148
  103.5 1.2 fusion.15
  104.7 0.7 convolution_convert_fusion
  105.5 41.2 %all_to_all.25 = bf16[8,512,256]{2,1,0:T(8,128)(2,1)S(1)} all-to-all(bf16[8,512,256]{2,1,0:T(8,128)(2,1)S(1)} %bitcast.83), channel_id=1, replica_groups=mesh['rep'=2,'fs_0'=4,'fs_1'=4,'tp'=8] {'tp'}, dimensions={0} | all-to-all | bytes 4194304 | tf_op jit(solution)/shard_map/all_to_all | solution.py:45
  147.0 0.6 copy-done.2
  147.9 1.5 broadcast_in_dim.22
  149.3 4.7 %all-to-all-start.3 = ((bf16[8,512,256]{1,2,0:T(8,128)(2,1)}), bf16[8,512,256]{1,2,0:T(8,128)(2,1)S(1)}, u32[]{:S(2)}, u32[]{:S(2)}) async-start(bf16[8,512,256]{1,2,0:T(8,128)(2,1)} %broadcast_in_dim.22), calls=%async_computation.3 | async-start | bytes 4194304 | tf_op jit(solution)/shard_map/all_to_all | solution.py:22
  154.1 4.0 %copy.49 = bf16[4,4,768,128]{3,2,1,0:T(8,128)(2,1)} copy(bf16[4,4,768,128]{3,2,0,1:T(8,128)(2,1)} %bitcast.93) | data formatting | bytes 6291456 | tf_op jit(solution)/shard_map/transpose | solution.py:56
  158.1 4.7 %copy.50 = bf16[768,16,128]{0,2,1:T(8,128)(2,1)} copy(bf16[768,16,128]{2,0,1:T(8,128)(2,1)} %bitcast.81) | data formatting | bytes 6291456 | tf_op jit(solution)/shard_map/transpose | solution.py:17
  162.8 23.3 %all-gather.8.cloned.1.call-done = bf16[16,128,768]{2,1,0:T(8,128)(2,1)} async-done(((bf16[4,128,768]{2,1,0:T(8,128)(2,1)}), bf16[16,128,768]{2,1,0:T(8,128)(2,1)}) %all-gather.8.cloned.1.call-update) | async-done | bytes 3145744 | tf_op jit(solution)/shard_map/all_gather | solution.py:52
  186.1 3.9 %copy.48 = bf16[4,4,128,768]{3,2,1,0:T(8,128)(2,1)} copy(bf16[4,4,128,768]{3,2,0,1:T(8,128)(2,1)} %bitcast.94) | data formatting | bytes 6291456 | tf_op jit(solution)/shard_map/transpose | solution.py:56
  190.0 0.5 fusion
  190.5 1.9 fusion.2
  192.4 7.6 %convolution_convert_fusion.1 = bf16[512,2048]{1,0:T(8,128)(2,1)S(1)} fusion(bf16[768,2048]{0,1:T(8,128)(2,1)} %bitcast.95, bf16[512,2048]{0,1:T(8,128)(2,1)} %bitcast.101, bf16[2048,768]{1,0:T(8,128)(2,1)} %bitcast.96), kind=kOutput, calls=%fused_computation.12 | convolution fusion | flops 3223453696 | bytes 10485760 | tf_op jit(solution)/shard_map/dot_general | solution.py:175
  200.1 31.1 %all_to_all.26 = bf16[8,512,256]{2,1,0:T(8,128)(2,1)S(1)} all-to-all(bf16[8,512,256]{2,1,0:T(8,128)(2,1)S(1)} %bitcast.84), channel_id=1, replica_groups=mesh['rep'=2,'fs_0'=4,'fs_1'=4,'tp'=8] {'tp'}, dimensions={0} | all-to-all | bytes 4194304 | tf_op jit(solution)/shard_map/all_to_all | solution.py:45
  231.5 0.8 add_convert_fusion
  (123 shorter events, 5.9 us)
Async XLA Ops:
  6.5 86.5 %copy-start = (bf16[4,64,64]{2,1,0:T(8,128)(2,1)S(1)}, bf16[4,64,64]{2,1,0:T(8,128)(2,1)}, u32[]{:S(2)}) copy-start(bf16[4,64,64]{2,1,0:T(8,128)(2,1)} %param.19) | copy-start | bytes 98308
  6.5 21.4 %copy-start.1 = (bf16[512,256]{1,0:T(8,128)(2,1)S(1)}, bf16[512,256]{1,0:T(8,128)(2,1)}, u32[]{:S(2)}) copy-start(bf16[512,256]{1,0:T(8,128)(2,1)} %param.13) | copy-start | bytes 786436
  6.5 83.2 %all-gather.6.cloned.1.call-start = ((), (), s32[]{:S(2)}) async-start(), calls=%async_computation.5 | async-start | bytes 2228224 | tf_op jit(solution)/shard_map/all_gather | solution.py:35
  8.1 145.9 %all-gather.10.cloned.1.call-start = ((), (), s32[]{:S(2)}) async-start(), calls=%async_computation.7 | async-start | bytes 3932160 | tf_op jit(solution)/shard_map/all_gather | solution.py:52
  29.6 8.2 %copy-start.3 = (bf16[128,768]{1,0:T(8,128)(2,1)S(1)}, bf16[128,768]{1,0:T(8,128)(2,1)}, u32[]{:S(2)}) copy-start(bf16[128,768]{1,0:T(8,128)(2,1)} %param.24) | copy-start | bytes 589828
  29.6 31.2 %copy-start.4 = (bf16[256,128]{1,0:T(8,128)(2,1)S(1)}, bf16[256,128]{1,0:T(8,128)(2,1)}, u32[]{:S(2)}) copy-start(bf16[256,128]{1,0:T(8,128)(2,1)} %param.23) | copy-start | bytes 196612
  29.6 31.3 %copy-start.8 = (f32[256]{0:T(256)S(1)}, f32[256]{0:T(256)}, u32[]{:S(2)}) copy-start(f32[256]{0:T(256)} %param.21) | copy-start | bytes 3076
  29.6 31.3 %copy-start.7 = (bf16[4,256]{1,0:T(4,128)(2,1)S(1)}, bf16[4,256]{1,0:T(4,128)(2,1)}, u32[]{:S(2)}) copy-start(bf16[4,256]{1,0:T(4,128)(2,1)} %param.18) | copy-start | bytes 6148
  29.6 34.5 %all-to-all-start = ((bf16[8,512,256]{1,2,0:T(8,128)(2,1)}), bf16[8,512,256]{1,2,0:T(8,128)(2,1)S(1)}, u32[]{:S(2)}, u32[]{:S(2)}) async-start(bf16[8,512,256]{1,2,0:T(8,128)(2,1)} %broadcast_in_dim.20), calls=%async_computation | async-start | bytes 4194304 | tf_op jit(solution)/shard_map/all_to_all | solution.py:22
  37.9 148.2 %all-gather.8.cloned.1.call-start = ((), (), s32[]{:S(2)}) async-start(), calls=%async_computation.6 | async-start | bytes 3932160 | tf_op jit(solution)/shard_map/all_gather | solution.py:52
  65.2 7.2 %copy-start.5 = (f32[2048]{0:T(1024)S(1)}, f32[2048]{0:T(1024)}, u32[]{:S(2)}) copy-start(f32[2048]{0:T(1024)} %param.14) | copy-start | bytes 24580
  65.3 39.4 %all-to-all-start.1 = ((bf16[16,256,128]{1,2,0:T(8,128)(2,1)}), bf16[16,256,128]{1,2,0:T(8,128)(2,1)S(1)}, u32[]{:S(2)}, u32[]{:S(2)}) async-start(bf16[16,256,128]{1,2,0:T(8,128)(2,1)} %broadcast_in_dim.21), calls=%async_computation.1 | async-start | bytes 2097152 | tf_op jit(solution)/shard_map/all_to_all | solution.py:22
  92.9 0.8 copy-start.9
  146.7 1.0 copy-start.2
  149.3 4.7 %copy-start.6 = (f32[2048]{0:T(1024)S(1)}, f32[2048]{0:T(1024)}, u32[]{:S(2)}) copy-start(f32[2048]{0:T(1024)} %param.15) | copy-start | bytes 24580
  149.3 40.6 %all-to-all-start.3 = ((bf16[8,512,256]{1,2,0:T(8,128)(2,1)}), bf16[8,512,256]{1,2,0:T(8,128)(2,1)S(1)}, u32[]{:S(2)}, u32[]{:S(2)}) async-start(bf16[8,512,256]{1,2,0:T(8,128)(2,1)} %broadcast_in_dim.22), calls=%async_computation.3 | async-start | bytes 4194304 | tf_op jit(solution)/shard_map/all_to_all | solution.py:22
Sparse Core Ops, SparseCore 0:
  9.1 80.6 all-gather.5
  91.6 50.3 all-gather.9
  143.8 42.2 all-gather.7
where the time goes:
time: 240 us; the launch traced here: 239 us
  blocking collectives  115 us (48%)
  waiting for transfers between devices  41.9 us (17%)
  local copies, waits for them, and re-layouts  22.1 us (9%)
  starting transfers between devices  19.6 us (8%)
  matrix products  14.3 us (6%)
  between operations  13.8 us (6%)
  other arithmetic  12.3 us (5%)
    all_to_all x2, blocking collectives, sent_and_summed(): lax.all_to_all(pieces, axis, split_axis=0, concat_axis=0, tiled=True)  72.2 us
    all_gather x2, blocking collectives, gather_in_order(): pieces = lax.all_gather(pieces, axes[k], axis=0, tiled=True)  42.6 us
    all_gather x2, waiting for transfers between devices, gather_in_order(): pieces = lax.all_gather(pieces, axes[k], axis=0, tiled=True)  23.3 us
    all_to_all x3, starting transfers between devices, from_everyone(): return lax.all_to_all(copies, axis, split_axis=0, concat_axis=0, tiled=True)  19.6 us
    all_gather x1, waiting for transfers between devices, in_one_piece(): lax.all_gather(both, axis, axis=dim, tiled=True)  15.4 us
    transpose x2, local copies, waits for them, and re-layouts, gather_in_order(): pieces.transpose(*turned, *range(len(order), pieces.ndim))  7.9 us
    dot_general x1, matrix products, shards(): jnp.dot(activity, gather_axes(down_projection_weight, FS, (0, 1), 1), pre...  7.6 us
  transfers between devices with their start and end apart: 6, of which 3 were waited for; matrix products, arithmetic and copies ran while one was open for 15% of the time, Pallas kernels for 0%

commit v1 on v0

--- a/solution.py
+++ b/solution.py
@@ -49,7 +49,16 @@
 def gather_in_order(value, axes, order):
     pieces = value[None]
     for k in order:
-        pieces = lax.all_gather(pieces, axes[k], axis=0, tiled=True)
+        message = axes[k]
+        pieces = jnp.concatenate(
+            lax.all_to_all(
+                jnp.stack(tuple((pieces for _ in range(lax.axis_size(message)))), axis=0),
+                message,
+                0,
+                0,
+            ),
+            0,
+        )
     held = [lax.axis_size(axes[k]) for k in reversed(order)]
     pieces = pieces.reshape(*held, *value.shape)
     turned = sorted(range(len(order)), key=lambda place: order[len(order) - 1 - place])

time: 240 us -> 352 us (1.47)
  waiting for transfers between devices: 41.9 us -> 126 us
  blocking collectives: 115 us -> 80.2 us
  local copies, waits for them, and re-layouts: 22.1 us -> 56.7 us
  starting transfers between devices: 19.6 us -> 33.8 us
  other arithmetic: 12.3 us -> 23.4 us
    all_to_all x3, waiting for transfers between devices: 3.17 us -> 49.5 us  [from_everyone(): return lax.all_to_all(copies, axis, split_axis=0, concat_axis=0, tiled=True)]
    all_gather x2 -> x0, blocking collectives: 42.6 us -> none  [gather_in_order(): pieces = lax.all_gather(pieces, axes[k], axis=0, tiled=True)]
    all_to_all x0 -> x4, waiting for transfers between devices: none -> 41 us  [gather_in_order(): lax.all_to_all(jnp.stack(tuple((pieces for _ in range(lax.axis_size(messa...]
    all_gather x2 -> x0, waiting for transfers between devices: 23.3 us -> none  [gather_in_order(): pieces = lax.all_gather(pieces, axes[k], axis=0, tiled=True)]
    all_gather x1, waiting for transfers between devices: 15.4 us -> 35.5 us  [in_one_piece(): lax.all_gather(both, axis, axis=dim, tiled=True)]
    all_to_all x0 -> x4, starting transfers between devices: none -> 16.2 us  [gather_in_order(): lax.all_to_all(jnp.stack(tuple((pieces for _ in range(lax.axis_size(messa...]
    pad x12, local copies, waits for them, and re-layouts: 0.74 us -> 13.3 us  [recurrent_states(): lax.associative_scan(combine, (jnp.exp(decay_logarithm).reshape(shaped),...]
    slice x39, local copies, waits for them, and re-layouts: 2.41 us -> 14.7 us  [recurrent_states(): lax.associative_scan(combine, (jnp.exp(decay_logarithm).reshape(shaped),...]
  transfers between devices with their start and end apart: 6 -> 8, of which waited for: 3 -> 6; matrix products, arithmetic and copies ran while one was open for 15% -> 21% of each run, Pallas kernels for 0% -> 0%
where the time goes in v1:
time: 352 us; the launch traced here: 349 us
  waiting for transfers between devices  126 us (36%)
  blocking collectives  80.2 us (23%)
  local copies, waits for them, and re-layouts  56.7 us (16%)
  starting transfers between devices  33.8 us (10%)
  other arithmetic  23.4 us (7%)
  matrix products  15 us (4%)
  between operations  14 us (4%)
    all_to_all x2, blocking collectives, sent_and_summed(): lax.all_to_all(pieces, axis, split_axis=0, concat_axis=0, tiled=True)  80.2 us
    all_to_all x3, waiting for transfers between devices, from_everyone(): return lax.all_to_all(copies, axis, split_axis=0, concat_axis=0, tiled=True)  49.5 us
    all_to_all x4, waiting for transfers between devices, gather_in_order(): lax.all_to_all(jnp.stack(tuple((pieces for _ in range(lax.axis_size(messa...  41 us
    all_gather x1, waiting for transfers between devices, in_one_piece(): lax.all_gather(both, axis, axis=dim, tiled=True)  35.5 us
    all_to_all x3, starting transfers between devices, from_everyone(): return lax.all_to_all(copies, axis, split_axis=0, concat_axis=0, tiled=True)  17.6 us
    all_to_all x4, starting transfers between devices, gather_in_order(): lax.all_to_all(jnp.stack(tuple((pieces for _ in range(lax.axis_size(messa...  16.2 us
    slice x39, local copies, waits for them, and re-layouts, recurrent_states(): lax.associative_scan(combine, (jnp.exp(decay_logarithm).reshape(shaped),...  14.7 us
    pad x12, local copies, waits for them, and re-layouts, recurrent_states(): lax.associative_scan(combine, (jnp.exp(decay_logarithm).reshape(shaped),...  13.3 us
  transfers between devices with their start and end apart: 8, of which 6 were waited for; matrix products, arithmetic and copies ran while one was open for 21% of the time, Pallas kernels for 0%

profile of v1, /device:TPU:1, one launch (start us, length us, event | category | flops | bytes accessed | tf_op | source)
XLA Modules:
  0.0 349.2 jit_solution(12796438874123091280)
XLA Ops:
  10.8 6.8 %all-to-all-start = ((bf16[8,512,256]{1,2,0:T(8,128)(2,1)}), bf16[8,512,256]{1,2,0:T(8,128)(2,1)S(1)}, u32[]{:S(2)}, u32[]{:S(2)}) async-start(bf16[8,512,256]{1,2,0:T(8,128)(2,1)} %broadcast_in_dim.6), calls=%async_computation | async-start | bytes 4194304 | tf_op jit(solution)/shard_map/all_to_all | solution.py:22
  17.8 26.2 %all-to-all-done = bf16[8,512,256]{1,2,0:T(8,128)(2,1)S(1)} async-done(((bf16[8,512,256]{1,2,0:T(8,128)(2,1)}), bf16[8,512,256]{1,2,0:T(8,128)(2,1)S(1)}, u32[]{:S(2)}, u32[]{:S(2)}) %all-to-all-start) | async-done | bytes 2097184 | tf_op jit(solution)/shard_map/all_to_all | solution.py:22
  44.9 4.6 %all-to-all-start.4 = ((bf16[4,1,128,768]{3,2,1,0:T(8,128)(2,1)}), bf16[4,1,128,768]{3,2,1,0:T(8,128)(2,1)S(1)}, u32[]{:S(2)}, u32[]{:S(2)}) async-start(bf16[4,1,128,768]{3,2,1,0:T(8,128)(2,1)} %stack.12), calls=%async_computation.4 | async-start | bytes 1572864 | tf_op jit(solution)/shard_map/all_to_all | solution.py:54
  50.0 1.9 fusion.4
  51.9 35.5 %all-gather.2.cloned.1.call-done = bf16[2048,512]{1,0:T(8,128)(2,1)} async-done(((bf16[128,512]{1,0:T(8,128)(2,1)}), bf16[2048,512]{1,0:T(8,128)(2,1)}) %all-gather.2.cloned.1.call-update) | async-done | bytes 2097168 | tf_op jit(solution)/shard_map/all_gather | solution.py:35
  87.4 2.6 convolution_convert_fusion.3
  91.2 3.5 %all-to-all-start.6 = ((bf16[4,1,768,128]{3,2,1,0:T(8,128)(2,1)}), bf16[4,1,768,128]{3,2,1,0:T(8,128)(2,1)S(1)}, u32[]{:S(2)}, u32[]{:S(2)}) async-start(bf16[4,1,768,128]{3,2,1,0:T(8,128)(2,1)} %stack.14), calls=%async_computation.6 | async-start | bytes 1572864 | tf_op jit(solution)/shard_map/all_to_all | solution.py:54
  99.1 7.5 %all-to-all-done.6 = bf16[4,1,768,128]{3,2,1,0:T(8,128)(2,1)S(1)} async-done(((bf16[4,1,768,128]{3,2,1,0:T(8,128)(2,1)}), bf16[4,1,768,128]{3,2,1,0:T(8,128)(2,1)S(1)}, u32[]{:S(2)}, u32[]{:S(2)}) %all-to-all-start.6) | async-done | bytes 786464 | tf_op jit(solution)/shard_map/all_to_all | solution.py:54
  107.7 4.9 %all-to-all-start.1 = ((bf16[16,256,128]{1,2,0:T(8,128)(2,1)}), bf16[16,256,128]{1,2,0:T(8,128)(2,1)S(1)}, u32[]{:S(2)}, u32[]{:S(2)}) async-start(bf16[16,256,128]{1,2,0:T(8,128)(2,1)} %broadcast_in_dim.7), calls=%async_computation.1 | async-start | bytes 2097152 | tf_op jit(solution)/shard_map/all_to_all | solution.py:22
  114.6 1.8 pad.51
  116.5 3.3 convolution_convert_fusion.2
  119.8 9.5 %all-to-all-done.1 = bf16[16,256,128]{1,2,0:T(8,128)(2,1)S(1)} async-done(((bf16[16,256,128]{1,2,0:T(8,128)(2,1)}), bf16[16,256,128]{1,2,0:T(8,128)(2,1)S(1)}, u32[]{:S(2)}, u32[]{:S(2)}) %all-to-all-start.1) | async-done | bytes 1048608 | tf_op jit(solution)/shard_map/all_to_all | solution.py:22
  129.3 2.2 stack.15
  131.5 3.7 %all-to-all-start.7 = ((bf16[4,4,768,128]{3,2,1,0:T(8,128)(2,1)}), bf16[4,4,768,128]{3,2,1,0:T(8,128)(2,1)S(1)}, u32[]{:S(2)}, u32[]{:S(2)}) async-start(bf16[4,4,768,128]{3,2,1,0:T(8,128)(2,1)} %stack.15), calls=%async_computation.7 | async-start | bytes 6291456 | tf_op jit(solution)/shard_map/all_to_all | solution.py:54
  139.7 1.7 slice.238
  156.1 3.5 %pad.59 = f32[4,64,256]{2,1,0:T(8,128)} pad(f32[4,32,256]{2,1,0:T(8,128)} %add.167, f32[]{:T(128)} %constant.34.clone.1), padding=0_0_0x1_0_1x0_0_0 | pad | bytes 393220 | tf_op jit(solution)/shard_map/pad | solution.py:128
  162.5 2.2 pad.60
  164.8 3.9 %pad.61 = f32[4,128,256]{2,1,0:T(8,128)} pad(f32[4,64,256]{2,1,0:T(8,128)} %add.169, f32[]{:T(128)} %constant.34.clone.1), padding=0_0_0x1_0_1x0_0_0 | pad | bytes 786436 | tf_op jit(solution)/shard_map/pad | solution.py:128
  173.4 50.5 %all_to_all.45 = bf16[8,512,256]{2,1,0:T(8,128)(2,1)} all-to-all(bf16[8,512,256]{2,1,0:T(8,128)(2,1)} %bitcast.80), channel_id=1, replica_groups=mesh['rep'=2,'fs_0'=4,'fs_1'=4,'tp'=8] {'tp'}, dimensions={0} | all-to-all | bytes 4194304 | tf_op jit(solution)/shard_map/all_to_all | solution.py:45
  223.9 2.0 stack.13
  226.0 4.5 %all-to-all-start.5 = ((bf16[4,4,128,768]{3,2,1,0:T(8,128)(2,1)}), bf16[4,4,128,768]{3,2,1,0:T(8,128)(2,1)S(1)}, u32[]{:S(2)}, u32[]{:S(2)}) async-start(bf16[4,4,128,768]{3,2,1,0:T(8,128)(2,1)} %stack.13), calls=%async_computation.5 | async-start | bytes 6291456 | tf_op jit(solution)/shard_map/all_to_all | solution.py:54
  230.4 2.0 convert_reduce_fusion.1
  233.3 33.5 %all-to-all-done.5 = bf16[4,4,128,768]{3,2,1,0:T(8,128)(2,1)S(1)} async-done(((bf16[4,4,128,768]{3,2,1,0:T(8,128)(2,1)}), bf16[4,4,128,768]{3,2,1,0:T(8,128)(2,1)S(1)}, u32[]{:S(2)}, u32[]{:S(2)}) %all-to-all-start.5) | async-done | bytes 3145760 | tf_op jit(solution)/shard_map/all_to_all | solution.py:54
  266.8 2.6 broadcast_in_dim.16
  269.4 5.8 %all-to-all-start.3 = ((bf16[8,512,256]{1,2,0:T(8,128)(2,1)}), bf16[8,512,256]{1,2,0:T(8,128)(2,1)S(1)}, u32[]{:S(2)}, u32[]{:S(2)}) async-start(bf16[8,512,256]{1,2,0:T(8,128)(2,1)} %broadcast_in_dim.16), calls=%async_computation.3 | async-start | bytes 4194304 | tf_op jit(solution)/shard_map/all_to_all | solution.py:22
  275.2 3.9 %copy.38 = bf16[4,4,768,128]{3,2,0,1:T(8,128)(2,1)} copy(bf16[4,4,768,128]{3,2,1,0:T(8,128)(2,1)} %copy-done.2) | data formatting | bytes 6291456 | tf_op jit(solution)/shard_map/all_to_all | solution.py:54
  279.1 4.7 %copy.39 = bf16[768,16,128]{0,2,1:T(8,128)(2,1)} copy(bf16[768,16,128]{2,0,1:T(8,128)(2,1)} %bitcast.79) | data formatting | bytes 6291456 | tf_op jit(solution)/shard_map/transpose | solution.py:17
  283.8 3.9 %copy.37 = bf16[4,4,128,768]{3,2,0,1:T(8,128)(2,1)} copy(bf16[4,4,128,768]{3,2,1,0:T(8,128)(2,1)} %copy-done.3) | data formatting | bytes 6291456 | tf_op jit(solution)/shard_map/all_to_all | solution.py:54
  287.6 13.8 %all-to-all-done.3 = bf16[8,512,256]{1,2,0:T(8,128)(2,1)S(1)} async-done(((bf16[8,512,256]{1,2,0:T(8,128)(2,1)}), bf16[8,512,256]{1,2,0:T(8,128)(2,1)S(1)}, u32[]{:S(2)}, u32[]{:S(2)}) %all-to-all-start.3) | async-done | bytes 2097184 | tf_op jit(solution)/shard_map/all_to_all | solution.py:22
  302.0 1.9 fusion.2
  303.8 7.6 %convolution_convert_fusion.1 = bf16[512,2048]{1,0:T(8,128)(2,1)S(1)} fusion(bf16[768,2048]{0,1:T(8,128)(2,1)} %bitcast.91, bf16[512,2048]{0,1:T(8,128)(2,1)} %bitcast.97, bf16[2048,768]{1,0:T(8,128)(2,1)} %bitcast.92), kind=kOutput, calls=%fused_computation.12 | convolution fusion | flops 3223453696 | bytes 10485760 | tf_op jit(solution)/shard_map/dot_general | solution.py:184
  311.6 29.7 %all_to_all.46 = bf16[8,512,256]{2,1,0:T(8,128)(2,1)S(1)} all-to-all(bf16[8,512,256]{2,1,0:T(8,128)(2,1)S(1)} %bitcast.82), channel_id=1, replica_groups=mesh['rep'=2,'fs_0'=4,'fs_1'=4,'tp'=8] {'tp'}, dimensions={0} | all-to-all | bytes 4194304 | tf_op jit(solution)/shard_map/all_to_all | solution.py:45
  (159 shorter events, 43.5 us)
Async XLA Ops:
  6.5 88.7 %copy-start = (bf16[4,64,64]{2,1,0:T(8,128)(2,1)S(1)}, bf16[4,64,64]{2,1,0:T(8,128)(2,1)}, u32[]{:S(2)}) copy-start(bf16[4,64,64]{2,1,0:T(8,128)(2,1)} %param.20) | copy-start | bytes 98308
  6.5 80.9 %all-gather.2.cloned.1.call-start = ((), (), s32[]{:S(2)}) async-start(), calls=%async_computation.9 | async-start | bytes 2228224 | tf_op jit(solution)/shard_map/all_gather | solution.py:35
  10.7 6.9 %copy-start.18 = (bf16[256,128]{1,0:T(8,128)(2,1)S(1)}, bf16[256,128]{1,0:T(8,128)(2,1)}, u32[]{:S(2)}) copy-start(bf16[256,128]{1,0:T(8,128)(2,1)} %param.23) | copy-start | bytes 196612
  10.8 7.0 %copy-start.24 = (f32[256]{0:T(256)S(1)}, f32[256]{0:T(256)}, u32[]{:S(2)}) copy-start(f32[256]{0:T(256)} %param.21) | copy-start | bytes 3076
  10.8 7.0 %copy-start.23 = (bf16[4,256]{1,0:T(4,128)(2,1)S(1)}, bf16[4,256]{1,0:T(4,128)(2,1)}, u32[]{:S(2)}) copy-start(bf16[4,256]{1,0:T(4,128)(2,1)} %param.18) | copy-start | bytes 6148
  10.8 33.2 %copy-start.16 = (bf16[128,768]{1,0:T(8,128)(2,1)S(1)}, bf16[128,768]{1,0:T(8,128)(2,1)}, u32[]{:S(2)}) copy-start(bf16[128,768]{1,0:T(8,128)(2,1)} %param.24) | copy-start | bytes 589828
  10.8 33.2 %all-to-all-start = ((bf16[8,512,256]{1,2,0:T(8,128)(2,1)}), bf16[8,512,256]{1,2,0:T(8,128)(2,1)S(1)}, u32[]{:S(2)}, u32[]{:S(2)}) async-start(bf16[8,512,256]{1,2,0:T(8,128)(2,1)} %broadcast_in_dim.6), calls=%async_computation | async-start | bytes 4194304 | tf_op jit(solution)/shard_map/all_to_all | solution.py:22
  17.8 32.2 %copy-start.21 = (f32[2048]{0:T(1024)S(1)}, f32[2048]{0:T(1024)}, u32[]{:S(2)}) copy-start(f32[2048]{0:T(1024)} %param.14) | copy-start | bytes 24580
  44.9 45.1 %all-to-all-start.4 = ((bf16[4,1,128,768]{3,2,1,0:T(8,128)(2,1)}), bf16[4,1,128,768]{3,2,1,0:T(8,128)(2,1)S(1)}, u32[]{:S(2)}, u32[]{:S(2)}) async-start(bf16[4,1,128,768]{3,2,1,0:T(8,128)(2,1)} %stack.12), calls=%async_computation.4 | async-start | bytes 1572864 | tf_op jit(solution)/shard_map/all_to_all | solution.py:54
  51.9 38.2 %copy-start.17 = (bf16[768,128]{1,0:T(8,128)(2,1)S(1)}, bf16[768,128]{1,0:T(8,128)(2,1)}, u32[]{:S(2)}) copy-start(bf16[768,128]{1,0:T(8,128)(2,1)} %param.25) | copy-start | bytes 589828
  90.1 5.2 %copy-start.8 = (bf16[4,1,128,768]{3,2,1,0:T(8,128)(2,1)}, bf16[4,1,128,768]{3,2,1,0:T(8,128)(2,1)S(1)}, u32[]{:S(2)}) copy-start(bf16[4,1,128,768]{3,2,1,0:T(8,128)(2,1)S(1)} %all-to-all-done.4) | copy-start | bytes 2359300
  91.2 15.4 %all-to-all-start.6 = ((bf16[4,1,768,128]{3,2,1,0:T(8,128)(2,1)}), bf16[4,1,768,128]{3,2,1,0:T(8,128)(2,1)S(1)}, u32[]{:S(2)}, u32[]{:S(2)}) async-start(bf16[4,1,768,128]{3,2,1,0:T(8,128)(2,1)} %stack.14), calls=%async_computation.6 | async-start | bytes 1572864 | tf_op jit(solution)/shard_map/all_to_all | solution.py:54
  98.0 1.0 copy-start.7
  98.7 9.0 %copy-start.10 = (f32[4,64,256]{2,1,0:T(8,128)}, f32[4,64,256]{2,1,0:T(8,128)S(1)}, u32[]{:S(2)}) copy-start(f32[4,64,256]{2,1,0:T(8,128)S(1)} %get-tuple-element.7) | copy-start | bytes 786436
  107.7 21.5 %all-to-all-start.1 = ((bf16[16,256,128]{1,2,0:T(8,128)(2,1)}), bf16[16,256,128]{1,2,0:T(8,128)(2,1)S(1)}, u32[]{:S(2)}, u32[]{:S(2)}) async-start(bf16[16,256,128]{1,2,0:T(8,128)(2,1)} %broadcast_in_dim.7), calls=%async_computation.1 | async-start | bytes 2097152 | tf_op jit(solution)/shard_map/all_to_all | solution.py:22
  112.7 7.1 %copy-start.12 = (f32[4,32,256]{2,1,0:T(8,128)}, f32[4,32,256]{2,1,0:T(8,128)S(1)}, u32[]{:S(2)}) copy-start(f32[4,32,256]{2,1,0:T(8,128)S(1)} %get-tuple-element.10) | copy-start | bytes 393220
  112.7 7.0 %copy-start.13 = (f32[4,32,256]{2,1,0:T(8,128)}, f32[4,32,256]{2,1,0:T(8,128)S(1)}, u32[]{:S(2)}) copy-start(f32[4,32,256]{2,1,0:T(8,128)S(1)} %get-tuple-element.9) | copy-start | bytes 393220
  113.0 6.8 %copy-start.15 = (f32[4,8,256]{2,1,0:T(8,128)}, f32[4,8,256]{2,1,0:T(8,128)S(1)}, u32[]{:S(2)}) copy-start(f32[4,8,256]{2,1,0:T(8,128)S(1)} %get-tuple-element.14) | copy-start | bytes 98308
  129.3 2.2 copy-start.4
  131.5 41.9 %all-to-all-start.7 = ((bf16[4,4,768,128]{3,2,1,0:T(8,128)(2,1)}), bf16[4,4,768,128]{3,2,1,0:T(8,128)(2,1)S(1)}, u32[]{:S(2)}, u32[]{:S(2)}) async-start(bf16[4,4,768,128]{3,2,1,0:T(8,128)(2,1)} %stack.15), calls=%async_computation.7 | async-start | bytes 6291456 | tf_op jit(solution)/shard_map/all_to_all | solution.py:54
  149.7 4.2 %copy-start.20 = (f32[4,1,256]{2,1,0:T(1,128)S(1)}, f32[4,1,256]{2,1,0:T(1,128)}, u32[]{:S(2)}) copy-start(f32[4,1,256]{2,1,0:T(1,128)} %slice.244) | copy-start | bytes 12292
  152.1 10.4 %copy-start.19 = (f32[4,1,256]{2,1,0:T(1,128)S(1)}, f32[4,1,256]{2,1,0:T(1,128)}, u32[]{:S(2)}) copy-start(f32[4,1,256]{2,1,0:T(1,128)} %slice.243) | copy-start | bytes 12292
  164.8 5.2 %copy-start.14 = (bf16[512,256]{1,0:T(8,128)(2,1)S(1)}, bf16[512,256]{1,0:T(8,128)(2,1)}, u32[]{:S(2)}) copy-start(bf16[512,256]{1,0:T(8,128)(2,1)} %convolution_convert_fusion.2) | copy-start | bytes 786436
  168.6 2.5 copy-start.5
  173.4 50.5 %copy-start.2 = (bf16[4,4,768,128]{3,2,1,0:T(8,128)(2,1)}, bf16[4,4,768,128]{3,2,1,0:T(8,128)(2,1)S(1)}, u32[]{:S(2)}) copy-start(bf16[4,4,768,128]{3,2,1,0:T(8,128)(2,1)S(1)} %all-to-all-done.7) | copy-start | bytes 9437188
  173.4 50.5 %copy-start.9 = (bf16[4,1,128,768]{3,2,1,0:T(8,128)(2,1)S(1)}, bf16[4,1,128,768]{3,2,1,0:T(8,128)(2,1)}, u32[]{:S(2)}) copy-start(bf16[4,1,128,768]{3,2,1,0:T(8,128)(2,1)} %copy-done.8) | copy-start | bytes 2359300
  226.0 40.8 %all-to-all-start.5 = ((bf16[4,4,128,768]{3,2,1,0:T(8,128)(2,1)}), bf16[4,4,128,768]{3,2,1,0:T(8,128)(2,1)S(1)}, u32[]{:S(2)}, u32[]{:S(2)}) async-start(bf16[4,4,128,768]{3,2,1,0:T(8,128)(2,1)} %stack.13), calls=%async_computation.5 | async-start | bytes 6291456 | tf_op jit(solution)/shard_map/all_to_all | solution.py:54
  230.4 2.0 copy-start.11
  266.8 2.6 copy-start.3
  269.4 5.8 %copy-start.22 = (f32[2048]{0:T(1024)S(1)}, f32[2048]{0:T(1024)}, u32[]{:S(2)}) copy-start(f32[2048]{0:T(1024)} %param.15) | copy-start | bytes 24580
  269.4 32.0 %all-to-all-start.3 = ((bf16[8,512,256]{1,2,0:T(8,128)(2,1)}), bf16[8,512,256]{1,2,0:T(8,128)(2,1)S(1)}, u32[]{:S(2)}, u32[]{:S(2)}) async-start(bf16[8,512,256]{1,2,0:T(8,128)(2,1)} %broadcast_in_dim.16), calls=%async_computation.3 | async-start | bytes 4194304 | tf_op jit(solution)/shard_map/all_to_all | solution.py:22
  311.6 30.8 %copy-start.1 = (bf16[4,64,64]{2,1,0:T(8,128)(2,1)S(1)}, bf16[4,64,64]{2,1,0:T(8,128)(2,1)}, u32[]{:S(2)}) copy-start(bf16[4,64,64]{2,1,0:T(8,128)(2,1)} %param.20) | copy-start | bytes 98308
  (2 other events, 1.7 us)
Sparse Core Ops, SparseCore 0:
  9.1 78.2 all-gather.1
